TPU v7x, 512 devices: a whole 4x4x16 slice. The times are simulated.
512 devices in a mesh: sp: 16 (over z), fs: 4 (over y), tp: 8 (over x, core).
Axes of the slice: x: 4, y: 4, z: 16, core: 2. Of those that a mesh axis runs over, the one named last changes fastest.
Arguments:
- inputs: bfloat16 [4, 4096, 4096], P('fs', 'sp', 'tp'), may hold values from -6 to 6
- norm_gain: float32 [4096], replicated, may hold values from 0.1 to 1.9
- conv_in_a: bfloat16 [4096, 1024], P(('sp', 'fs'), 'tp'), may hold values from -0.09375 to 0.09375
- conv_in_b: bfloat16 [4096, 1024], P(('sp', 'fs'), 'tp'), may hold values from -0.09375 to 0.09375
- query_w: bfloat16 [4096, 512], P(('sp', 'fs'), 'tp'), may hold values from -0.09375 to 0.09375
- key_w: bfloat16 [4096, 512], P(('sp', 'fs'), 'tp'), may hold values from -0.09375 to 0.09375
- value_w: bfloat16 [4096, 1024], P(('sp', 'fs'), 'tp'), may hold values from -0.09375 to 0.09375
- out_gate_w: bfloat16 [4096, 1024], P(('sp', 'fs'), 'tp'), may hold values from -0.09375 to 0.09375
- pointwise_w: bfloat16 [4096, 1024], P(('sp', 'fs'), 'tp'), may hold values from -0.1875 to 0.1875
- gla_out_w: bfloat16 [4096, 1024], P(('sp', 'fs'), 'tp'), may hold values from -0.1875 to 0.1875
- forget_first_factor: bfloat16 [4096, 64], replicated, may hold values from -0.09375 to 0.09375
- decay_w: bfloat16 [64, 512], replicated, may hold values from -0.75 to 0.75
- decay_bias: float32 [512], replicated, as said below
- decay_extra: float32 [4, 4096, 512], P('fs', 'sp', 'tp'), may hold values from -2.2 to 0, as said below
- conv_kernel: float32 [31, 1024], replicated, may hold values from -7 to 7
- conv_gain: float32 [1024], replicated, may hold values from 0.1 to 1.9
- head_gain: float32 [64], replicated, may hold values from 0.1 to 1.9
Outputs:
- mixed: bfloat16 [4, 4096, 4096], P('fs', 'sp', 'tp')
Inputs may be any that keep to these rules, and one draw needn't show every extreme that they name: decay_bias is positive. decay_extra is never positive.
All inputs are finite; a program needn't handle non-finite values.
Results may differ from a plain program's by a relative error of at most 0.015.
Values may be sent and summed in bfloat16 or wider, within the bound.
A program may use at most 128 MiB of HBM per device.

v0:
```python
import jax
import jax.numpy as jnp
from jax import lax
from jax.sharding import PartitionSpec as P

DK = 32
DV = 64
BLOCK = 64


def side_by_side(arrays, axis, dim, along):
    ends, at = ([], 0)
    for a in arrays[:-1]:
        at += a.shape[along]
        ends.append(at)
    both = jnp.concatenate(arrays, axis=along)
    return tuple(jnp.split(lax.all_gather(both, axis, axis=dim, tiled=True), ends, axis=along))


def from_everyone(value, axis):
    length = lax.axis_size(axis)
    return lax.all_to_all(
        jnp.broadcast_to(value[None], (length, *value.shape)), axis, 0, 0, tiled=True
    )


def in_order(tiles, dim):
    lengths = list(tiles.shape[1:])
    lengths[dim] *= tiles.shape[0]
    return jnp.moveaxis(tiles, 0, dim).reshape(lengths)


def gathered_copies(value, axis, dim):
    tiles = from_everyone(value, axis)
    return in_order(tiles, dim)


def from_behind(value, axis, by):
    length = lax.axis_size(axis)
    pairs = [(i, i + by) for i in range(length) if 0 <= i + by < length]
    return lax.ppermute(value, axis, pairs)


def over_copies(value, axis):
    everything = from_everyone(value, axis)
    return jnp.sum(everything, axis=0)


def in_one(arrays, axis):
    vector, at, outs = (jnp.concatenate([a.reshape(-1) for a in arrays]), 0, [])
    subtotal = over_copies(vector, axis)
    for a in arrays:
        outs.append(subtotal[at : at + a.size].reshape(a.shape))
        at += a.size
    return tuple(outs)


def in_blocks(value, dim, length):
    lengths = value.shape
    tiles = value.reshape(*lengths[:dim], length, lengths[dim] // length, *lengths[dim + 1 :])
    return jnp.moveaxis(tiles, dim, 0)


def sum_at_owner(value, axis, dim):
    length = lax.axis_size(axis)
    tiles = lax.all_to_all(in_blocks(value, dim, length), axis, 0, 0, tiled=True)
    return jnp.sum(tiles.astype(jnp.float32), axis=0)


def shards(
    inputs,
    norm_gain,
    conv_in_a,
    conv_in_b,
    query_w,
    key_w,
    value_w,
    out_gate_w,
    pointwise_w,
    gla_out_w,
    forget_first_factor,
    decay_w,
    decay_bias,
    decay_extra,
    conv_kernel,
    conv_gain,
    head_gain,
):
    nearer = side_by_side(
        (conv_in_a, conv_in_b, query_w, key_w, value_w, out_gate_w, pointwise_w, gla_out_w),
        "fs",
        0,
        1,
    )
    collected = side_by_side(
        (nearer[0], nearer[1], nearer[2], nearer[3], nearer[4], nearer[5], nearer[6], nearer[7]),
        "sp",
        0,
        1,
    )
    (
        conv_a_full,
        conv_b_full,
        query_full,
        key_full,
        value_full,
        gate_full,
        pointwise_full,
        gla_out_full,
    ) = collected
    tok_rows = inputs[0]
    token_count = tok_rows.shape[0]
    in_weights = (
        conv_a_full,
        conv_b_full,
        query_full,
        key_full,
        value_full,
        gate_full,
        forget_first_factor,
    )
    segment_values = gathered_copies(tok_rows, "tp", 1).astype(jnp.float32)
    scaled = (segment_values * norm_gain).astype(jnp.bfloat16)
    sums = tuple(
        (jnp.dot(scaled, weight, preferred_element_type=jnp.float32) for weight in in_weights)
    )
    sums, squares = (sums, jnp.sum(segment_values * segment_values, axis=1))
    row_scale = lax.rsqrt(squares / norm_gain.shape[0] + 1e-06)[:, None]
    conv_a, conv_b, queries, keys, values, out_gate, low_rank = [
        (running * row_scale).astype(jnp.bfloat16) for running in sums
    ]
    gated = (conv_a.astype(jnp.float32) * jax.nn.sigmoid(conv_b.astype(jnp.float32))).astype(
        jnp.bfloat16
    )
    reach = conv_kernel.shape[0] - 1
    earlier = from_behind(gated[token_count - reach :], "sp", 1)
    extended = jnp.concatenate([earlier, gated], axis=0).astype(jnp.float32)
    tp_index = lax.axis_index("tp")
    channels = gated.shape[1]
    kernel = lax.dynamic_slice_in_dim(conv_kernel, tp_index * channels, channels, 1)
    convolved = jnp.zeros((token_count, channels), jnp.float32)
    for offset in range(reach + 1):
        convolved = convolved + kernel[offset] * extended[offset : offset + token_count]
    channel_sum, channel_squares = in_one(
        (jnp.sum(convolved, axis=1), jnp.sum(convolved * convolved, axis=1)), "tp"
    )
    total_channels = conv_gain.shape[0]
    average = channel_sum / total_channels
    spread_squared_mean = channel_squares / total_channels - average * average
    gain_part = lax.dynamic_slice_in_dim(conv_gain, tp_index * channels, channels)
    normed = (
        (convolved - average[:, None]) * lax.rsqrt(spread_squared_mean + 1e-05)[:, None] * gain_part
    )
    conv_act = jax.nn.silu(normed).astype(jnp.bfloat16)
    key_width = keys.shape[1]
    head_count = key_width // DK
    decay_part = lax.dynamic_slice_in_dim(decay_w, tp_index * key_width, key_width, 1)
    bias_part = lax.dynamic_slice_in_dim(decay_bias, tp_index * key_width, key_width)
    pre_decay = jnp.dot(low_rank, decay_part, preferred_element_type=jnp.float32) + bias_part
    log_decay = jax.nn.log_sigmoid(pre_decay) / 16.0 + decay_extra[0]
    block_count = token_count // BLOCK
    highest = lax.Precision.HIGHEST

    def split_blocks(array_operand, width):
        return array_operand.reshape(block_count, BLOCK, head_count, width).transpose(0, 2, 1, 3)

    q_blocks = split_blocks(queries.astype(jnp.float32), DK) * DK ** (-0.5)
    k_blocks = split_blocks(keys.astype(jnp.float32), DK)
    v_blocks = split_blocks(values.astype(jnp.float32), DV)
    prefix_running_sum = jnp.cumsum(split_blocks(log_decay, DK), axis=2)
    causal = jnp.tril(jnp.ones((BLOCK, BLOCK), dtype=bool))
    spread = prefix_running_sum[:, :, :, None, :] - prefix_running_sum[:, :, None, :, :]
    weights_in = jnp.exp(jnp.where(causal[:, :, None], spread, -jnp.inf))
    scores = jnp.einsum("nhid,nhjd,nhijd->nhij", q_blocks, k_blocks, weights_in, precision=highest)
    inner = jnp.einsum("nhij,nhjv->nhiv", scores, v_blocks, precision=highest)
    block_total = prefix_running_sum[:, :, -1]
    block_state = jnp.einsum(
        "nhjd,nhjv->nhdv",
        k_blocks * jnp.exp(block_total[:, :, None] - prefix_running_sum),
        v_blocks,
        precision=highest,
    )

    def advance(state, block_pair):
        decay_row, added_share_term = block_pair
        return (jnp.exp(decay_row)[..., None] * state + added_share_term, state)

    local_final, local_entering = lax.scan(
        advance, jnp.zeros((head_count, DK, DV), jnp.float32), (block_total, block_state)
    )
    device_total = jnp.sum(block_total, axis=0)
    totals = lax.all_gather(device_total[None], "sp", axis=0, tiled=True)
    running_totals = jnp.cumsum(totals, axis=0)
    sp_index = lax.axis_index("sp")
    before = lax.dynamic_index_in_dim(
        running_totals, sp_index, 0, False
    ) - lax.dynamic_index_in_dim(totals, sp_index, 0, False)
    piece = lax.all_gather(local_final[None], "sp", axis=0, tiled=True)
    number = piece.shape[0]
    anchor = jnp.arange(number, dtype=jnp.int32)
    exponent = jnp.where(
        (anchor < sp_index)[:, None, None], before[None] - running_totals, -jnp.inf
    )
    entering = jnp.einsum("nhd,nhdv->hdv", jnp.exp(exponent), piece, precision=highest)
    passed = jnp.exp(jnp.cumsum(block_total, axis=0) - block_total)
    entering_blocks = passed[..., None] * entering[None] + local_entering
    outer = jnp.einsum(
        "nhid,nhdv->nhiv",
        q_blocks * jnp.exp(prefix_running_sum),
        entering_blocks,
        precision=highest,
    )
    head_output = inner + outer
    normed_heads = (
        head_output
        * lax.rsqrt(jnp.mean(head_output * head_output, axis=-1, keepdims=True) + 1e-06)
        * head_gain
    )
    gla_rows = normed_heads.transpose(0, 2, 1, 3).reshape(token_count, head_count * DV)
    gla_act = (gla_rows * jax.nn.silu(out_gate.astype(jnp.float32))).astype(jnp.bfloat16)
    contract = (((1,), (1,)), ((), ()))
    conv_term = lax.dot_general(
        pointwise_full, conv_act, contract, preferred_element_type=jnp.float32
    )
    summed = sum_at_owner(
        (
            conv_term
            + lax.dot_general(gla_out_full, gla_act, contract, preferred_element_type=jnp.float32)
        ).astype(jnp.bfloat16),
        "tp",
        0,
    )
    return (tok_rows.astype(jnp.float32) + summed.T).astype(jnp.bfloat16)[None]


def solution(mesh):
    return jax.shard_map(
        shards,
        mesh=mesh,
        in_specs=(
            P("fs", "sp", "tp"),
            P(),
            P(("sp", "fs"), "tp"),
            P(("sp", "fs"), "tp"),
            P(("sp", "fs"), "tp"),
            P(("sp", "fs"), "tp"),
            P(("sp", "fs"), "tp"),
            P(("sp", "fs"), "tp"),
            P(("sp", "fs"), "tp"),
            P(("sp", "fs"), "tp"),
            P(),
            P(),
            P(),
            P("fs", "sp", "tp"),
            P(),
            P(),
            P(),
        ),
        out_specs=P("fs", "sp", "tp"),
        check_vma=False,
    )
```

profile of v0, /device:TPU:1, one launch (start us, length us, event | category | flops | bytes accessed | tf_op | source)
XLA Modules:
  0.0 245.8 jit_solution(409942196637541957)
XLA Ops:
  6.5 1.0 concatenate.11
  7.5 12.3 %all_gather.12 = bf16[256,896]{1,0:T(8,128)(2,1)} all-gather(bf16[64,896]{1,0:T(8,128)(2,1)S(1)} %concatenate.11), channel_id=1, replica_groups=mesh['sp'=16,'fs'=4,'tp'=8] {'fs'}, dimensions={0}, use_global_device_ids=true | all-gather | bytes 573440 | tf_op jit(solution)/shard_map/all_gather | solution.py:17
  19.8 1.1 copy.64
  20.9 1.5 broadcast_in_dim.45
  22.4 11.6 %all-to-all-start = ((bf16[8,256,512]{1,2,0:T(8,128)(2,1)}), bf16[8,256,512]{1,2,0:T(8,128)(2,1)S(1)}, u32[]{:S(2)}, u32[]{:S(2)}) async-start(bf16[8,256,512]{1,2,0:T(8,128)(2,1)} %broadcast_in_dim.45), calls=%async_computation | async-start | bytes 4194304 | tf_op jit(solution)/shard_map/all_to_all | solution.py:22
  34.8 1.3 dynamic_slice.28
  36.1 1.7 dynamic-slice_bitcast_fusion.29
  37.8 1.9 fusion.98
  39.7 20.6 %all-to-all-done = bf16[8,256,512]{1,2,0:T(8,128)(2,1)S(1)} async-done(((bf16[8,256,512]{1,2,0:T(8,128)(2,1)}), bf16[8,256,512]{1,2,0:T(8,128)(2,1)S(1)}, u32[]{:S(2)}, u32[]{:S(2)}) %all-to-all-start) | async-done | bytes 2097184 | tf_op jit(solution)/shard_map/all_to_all | solution.py:22
  60.9 1.8 fusion.2
  62.6 2.2 fusion.86
  65.5 28.2 %all-gather.2 = f32[16,2,32]{2,1,0:T(2,128)S(1)} all-gather(f32[1,2,32]{2,1,0:T(2,128)S(1)} %bitcast.160), channel_id=2, replica_groups=mesh['sp'=16,'fs'=4,'tp'=8] {'sp'}, dimensions={0}, use_global_device_ids=true | all-gather | bytes 4352 | tf_op jit(solution)/shard_map/all_gather | solution.py:192
  94.0 4.6 %select_exponential_fusion = f32[4,2,64,64,32]{3,4,2,1,0:T(8,128)} fusion(f32[4,2,64,32]{2,3,1,0:T(8,128)S(1)} %copy.67, f32[4,2,64,32]{3,2,1,0:T(8,128)S(1)} %reduce_window_sum.35, pred[64,64]{1,0:T(8,128)(4,1)S(1)} %iota_compare_fusion), kind=kLoop, calls=%fused_computation.5 | loop fusion | flops 2097152 | bytes 4329472 | tf_op jit(solution)/shard_map/exp | solution.py:173
  98.5 11.0 %copy.82 = f32[4,2,64,64,32]{2,3,4,1,0:T(8,128)} copy(f32[4,2,64,64,32]{3,4,2,1,0:T(8,128)} %select_exponential_fusion) | data formatting | bytes 8388608
  109.6 12.5 %all-gather.5.cloned.1.call-done = bf16[4096,896]{1,0:T(8,128)(2,1)} async-done(((bf16[256,896]{1,0:T(8,128)(2,1)}), bf16[4096,896]{1,0:T(8,128)(2,1)}) %all-gather.5.cloned.1.call-update) | async-done | bytes 7340048 | tf_op jit(solution)/shard_map/all_gather | solution.py:17
  122.1 2.2 fusion.18
  125.3 2.0 fusion.13
  127.4 2.0 fusion.38
  129.4 5.8 %while.13 = (s32[]{:T(128)}, f32[2,32,64]{2,1,0:T(8,128)S(1)}, f32[4,2,32,64]{3,2,1,0:T(8,128)}, f32[4,2,32]{2,1,0:T(2,128)S(1)}, f32[4,2,32,64]{3,2,1,0:T(8,128)}, /*index=5*/s32[]{:T(128)}, s32[]{:T(128)}) while((s32[]{:T(128)}, f32[2,32,64]{2,1,0:T(8,128)S(1)}, f32[4,2,32,64]{3,2,1,0:T(8,128)}, f32[4,2,32]{2,1,0:T(2,128)S(1)}, ...), condition=%wide.region_9.10_spmd.clone, body=%wide.region_8.9_spmd.clone.sunk | while | flops 16387 | bytes 99680 | solution.py:188
  135.2 25.9 %all-gather.1 = f32[32,32,64]{2,1,0:T(8,128)} all-gather(f32[2,32,64]{2,1,0:T(8,128)S(1)} %get-tuple-element.33), channel_id=3, replica_groups=mesh['sp'=16,'fs'=4,'tp'=8] {'sp'}, dimensions={0}, use_global_device_ids=true | all-gather | bytes 278528 | tf_op jit(solution)/shard_map/all_gather | solution.py:198
  161.7 1.8 fusion.21
  164.5 5.3 %fusion = f32[4,2,64,64]{2,3,1,0:T(8,128)S(1)} fusion(f32[4,2,64,64,32]{2,3,4,1,0:T(8,128)} %copy.82, f32[4,2,32,64]{3,2,1,0:T(8,128)S(1)} %copy.69, f32[4,2,32,64]{3,2,1,0:T(8,128)} %copy.68), kind=kLoop, calls=%fused_computation.4 | loop fusion | flops 3112960 | bytes 4456448 | tf_op jit(solution)/shard_map/nhid,nhjd,nhijd->nhij/dot_general | solution.py:174
  170.4 2.0 fusion.12
  172.4 2.0 fusion.6
  174.4 2.2 collective-permute-start
  176.7 0.9 fusion.34
  178.7 1.2 fusion.101
  180.4 12.4 %all-to-all-start.1 = ((f32[8,1,512]{2,1,0:T(1,128)}), f32[8,1,512]{2,1,0:T(1,128)S(1)}, u32[]{:S(2)}, u32[]{:S(2)}) async-start(f32[8,1,512]{2,1,0:T(1,128)} %broadcast_in_dim.46), calls=%async_computation.1 | async-start | bytes 32768 | tf_op jit(solution)/shard_map/all_to_all | solution.py:22
  194.0 3.6 %all-to-all-done.1 = f32[8,1,512]{2,1,0:T(1,128)S(1)} async-done(((f32[8,1,512]{2,1,0:T(1,128)}), f32[8,1,512]{2,1,0:T(1,128)S(1)}, u32[]{:S(2)}, u32[]{:S(2)}) %all-to-all-start.1) | async-done | bytes 16416 | tf_op jit(solution)/shard_map/all_to_all | solution.py:22
  197.6 4.1 %fusion.31 = f32[4096,256]{1,0:T(8,128)} fusion(bf16[4096,896]{1,0:T(8,128)(2,1)} %all-gather.5.cloned.1.call-done, f32[256,128]{1,0:T(8,128)} %get-tuple-element.65, f32[128]{0:T(128)} %dynamic_slice.28, f32[256]{0:T(256)S(1)} %get-tuple-element.100, f32[256]{0:T(256)S(1)} %get-tuple-element.99), kind=kOutput, calls=%fused_computation.50 | convolution fusion | flops 268697600 | bytes 5376512 | tf_op jit(solution)/shard_map/dot_general | solution.py:222
  201.7 5.7 %fusion.1 = bf16[4096,256]{1,0:T(8,128)(2,1)} fusion(f32[4096,256]{1,0:T(8,128)} %fusion.31, bf16[4096,896]{1,0:T(8,128)(2,1)} %all-gather.5.cloned.1.call-done, f32[256,128]{1,0:T(8,128)S(1)} %reshape.78, bf16[256,4096]{0,1:T(8,128)(2,1)S(1)} %copy-done.1, f32[256]{0:T(256)S(1)} %add_rsqrt_fusion.1), kind=kOutput, calls=%fused_computation.7 | convolution fusion | flops 539262976 | bytes 10617856 | tf_op jit(solution)/shard_map/dot_general | solution.py:228
  207.3 30.4 %all_to_all.16 = bf16[8,512,256]{2,1,0:T(8,128)(2,1)S(1)} all-to-all(bf16[8,512,256]{2,1,0:T(8,128)(2,1)} %bitcast.150), channel_id=1, replica_groups=mesh['sp'=16,'fs'=4,'tp'=8] {'tp'}, dimensions={0} | all-to-all | bytes 4194304 | tf_op jit(solution)/shard_map/all_to_all | solution.py:66
  (128 shorter events, 15.0 us)
Async XLA Ops:
  6.5 56.1 %copy-start = (bf16[4096,64]{0,1:T(8,128)(2,1)S(1)}, bf16[4096,64]{0,1:T(8,128)(2,1)}, u32[]{:S(2)}) copy-start(bf16[4096,64]{0,1:T(8,128)(2,1)} %param.29) | copy-start | bytes 1572868
  6.5 115.5 %all-gather.5.cloned.1.call-start = ((), (), s32[]{:S(2)}) async-start(), calls=%async_computation.3 | async-start | bytes 7798784 | tf_op jit(solution)/shard_map/all_gather | solution.py:17
  20.9 39.9 %copy-start.6 = (f32[4096]{0:T(1024)S(1)}, f32[4096]{0:T(1024)}, u32[]{:S(2)}) copy-start(f32[4096]{0:T(1024)} %param.20) | copy-start | bytes 49156
  22.4 37.8 %all-to-all-start = ((bf16[8,256,512]{1,2,0:T(8,128)(2,1)}), bf16[8,256,512]{1,2,0:T(8,128)(2,1)S(1)}, u32[]{:S(2)}, u32[]{:S(2)}) async-start(bf16[8,256,512]{1,2,0:T(8,128)(2,1)} %broadcast_in_dim.45), calls=%async_computation | async-start | bytes 4194304 | tf_op jit(solution)/shard_map/all_to_all | solution.py:22
  34.0 28.6 %copy-start.5 = (f32[1,256,64]{1,2,0:T(8,128)S(1)}, f32[1,256,64]{1,2,0:T(8,128)}, u32[]{:S(2)}) copy-start(f32[1,256,64]{1,2,0:T(8,128)} %param.32) | copy-start | bytes 196612
  98.5 23.5 %copy-start.1 = (bf16[256,4096]{0,1:T(8,128)(2,1)S(1)}, bf16[256,4096]{0,1:T(8,128)(2,1)}, u32[]{:S(2)}) copy-start(bf16[256,4096]{0,1:T(8,128)(2,1)} %fusion.2) | copy-start | bytes 6291460
  170.1 8.2 %copy-start.7 = (f32[128]{0:T(128)S(1)}, f32[128]{0:T(128)}, u32[]{:S(2)}) copy-start(f32[128]{0:T(128)} %get-tuple-element.69) | copy-start | bytes 1540
  170.1 8.2 %copy-start.8 = (f32[128]{0:T(128)S(1)}, f32[128]{0:T(128)}, u32[]{:S(2)}) copy-start(f32[128]{0:T(128)} %get-tuple-element.70) | copy-start | bytes 1540
  170.1 8.2 %copy-start.9 = (f32[128]{0:T(128)S(1)}, f32[128]{0:T(128)}, u32[]{:S(2)}) copy-start(f32[128]{0:T(128)} %get-tuple-element.71) | copy-start | bytes 1540
  170.2 8.2 %copy-start.10 = (f32[128]{0:T(128)S(1)}, f32[128]{0:T(128)}, u32[]{:S(2)}) copy-start(f32[128]{0:T(128)} %get-tuple-element.72) | copy-start | bytes 1540
  170.2 8.2 %copy-start.11 = (f32[128]{0:T(128)S(1)}, f32[128]{0:T(128)}, u32[]{:S(2)}) copy-start(f32[128]{0:T(128)} %get-tuple-element.73) | copy-start | bytes 1540
  170.2 8.2 %copy-start.12 = (f32[128]{0:T(128)S(1)}, f32[128]{0:T(128)}, u32[]{:S(2)}) copy-start(f32[128]{0:T(128)} %get-tuple-element.74) | copy-start | bytes 1540
  170.2 8.2 %copy-start.13 = (f32[128]{0:T(128)S(1)}, f32[128]{0:T(128)}, u32[]{:S(2)}) copy-start(f32[128]{0:T(128)} %get-tuple-element.75) | copy-start | bytes 1540
  170.2 8.2 %copy-start.14 = (f32[128]{0:T(128)S(1)}, f32[128]{0:T(128)}, u32[]{:S(2)}) copy-start(f32[128]{0:T(128)} %get-tuple-element.76) | copy-start | bytes 1540
  170.2 8.2 %copy-start.15 = (f32[128]{0:T(128)S(1)}, f32[128]{0:T(128)}, u32[]{:S(2)}) copy-start(f32[128]{0:T(128)} %get-tuple-element.77) | copy-start | bytes 1540
  170.2 8.2 %copy-start.16 = (f32[128]{0:T(128)S(1)}, f32[128]{0:T(128)}, u32[]{:S(2)}) copy-start(f32[128]{0:T(128)} %get-tuple-element.78) | copy-start | bytes 1540
  170.2 8.2 %copy-start.17 = (f32[128]{0:T(128)S(1)}, f32[128]{0:T(128)}, u32[]{:S(2)}) copy-start(f32[128]{0:T(128)} %get-tuple-element.79) | copy-start | bytes 1540
  170.2 8.2 %copy-start.18 = (f32[128]{0:T(128)S(1)}, f32[128]{0:T(128)}, u32[]{:S(2)}) copy-start(f32[128]{0:T(128)} %get-tuple-element.80) | copy-start | bytes 1540
  170.2 8.2 %copy-start.19 = (f32[128]{0:T(128)S(1)}, f32[128]{0:T(128)}, u32[]{:S(2)}) copy-start(f32[128]{0:T(128)} %get-tuple-element.81) | copy-start | bytes 1540
  170.3 8.2 %copy-start.20 = (f32[128]{0:T(128)S(1)}, f32[128]{0:T(128)}, u32[]{:S(2)}) copy-start(f32[128]{0:T(128)} %get-tuple-element.82) | copy-start | bytes 1540
  170.3 8.2 %copy-start.21 = (f32[128]{0:T(128)S(1)}, f32[128]{0:T(128)}, u32[]{:S(2)}) copy-start(f32[128]{0:T(128)} %get-tuple-element.83) | copy-start | bytes 1540
  170.3 8.2 %copy-start.22 = (f32[128]{0:T(128)S(1)}, f32[128]{0:T(128)}, u32[]{:S(2)}) copy-start(f32[128]{0:T(128)} %get-tuple-element.84) | copy-start | bytes 1540
  170.3 8.2 %copy-start.23 = (f32[128]{0:T(128)S(1)}, f32[128]{0:T(128)}, u32[]{:S(2)}) copy-start(f32[128]{0:T(128)} %get-tuple-element.85) | copy-start | bytes 1540
  170.3 8.2 %copy-start.24 = (f32[128]{0:T(128)S(1)}, f32[128]{0:T(128)}, u32[]{:S(2)}) copy-start(f32[128]{0:T(128)} %get-tuple-element.86) | copy-start | bytes 1540
  170.3 8.2 %copy-start.25 = (f32[128]{0:T(128)S(1)}, f32[128]{0:T(128)}, u32[]{:S(2)}) copy-start(f32[128]{0:T(128)} %get-tuple-element.87) | copy-start | bytes 1540
  170.3 8.2 %copy-start.26 = (f32[128]{0:T(128)S(1)}, f32[128]{0:T(128)}, u32[]{:S(2)}) copy-start(f32[128]{0:T(128)} %get-tuple-element.88) | copy-start | bytes 1540
  170.3 8.2 %copy-start.27 = (f32[128]{0:T(128)S(1)}, f32[128]{0:T(128)}, u32[]{:S(2)}) copy-start(f32[128]{0:T(128)} %get-tuple-element.89) | copy-start | bytes 1540
  170.3 8.2 %copy-start.28 = (f32[128]{0:T(128)S(1)}, f32[128]{0:T(128)}, u32[]{:S(2)}) copy-start(f32[128]{0:T(128)} %get-tuple-element.90) | copy-start | bytes 1540
  170.3 8.2 %copy-start.29 = (f32[128]{0:T(128)S(1)}, f32[128]{0:T(128)}, u32[]{:S(2)}) copy-start(f32[128]{0:T(128)} %get-tuple-element.91) | copy-start | bytes 1540
  170.4 8.2 %copy-start.30 = (f32[128]{0:T(128)S(1)}, f32[128]{0:T(128)}, u32[]{:S(2)}) copy-start(f32[128]{0:T(128)} %get-tuple-element.92) | copy-start | bytes 1540
  174.4 3.9 %collective-permute-start = (bf16[30,128]{1,0:T(8,128)(2,1)S(1)}, bf16[30,128]{1,0:T(8,128)(2,1)S(1)}, u32[]{:S(2)}, u32[]{:S(2)}) collective-permute-start(bf16[30,128]{1,0:T(8,128)(2,1)S(1)} %slice.265), channel_id=1, source_target_pairs={{0,32},{32,64},{64,96},{96,128},{128,160},{160,192},{192,224},{224... | collective-permute-start | bytes 23048 | tf_op jit(solution)/shard_map/ppermute | solution.py:41
  180.4 17.1 %all-to-all-start.1 = ((f32[8,1,512]{2,1,0:T(1,128)}), f32[8,1,512]{2,1,0:T(1,128)S(1)}, u32[]{:S(2)}, u32[]{:S(2)}) async-start(f32[8,1,512]{2,1,0:T(1,128)} %broadcast_in_dim.46), calls=%async_computation.1 | async-start | bytes 32768 | tf_op jit(solution)/shard_map/all_to_all | solution.py:22
  (9 other events, 71.2 us)
Sparse Core Ops, SparseCore 0:
  20.0 102.0 all-gather.4
where the time goes:
time: 247 us; the launch traced here: 246 us
  blocking collectives  96.8 us (39%)
  waiting for transfers between devices  36.6 us (15%)
  starting transfers between devices  26.3 us (11%)
  matrix products  25.9 us (10%)
  local copies, waits for them, and re-layouts  25.3 us (10%)
  other arithmetic  20.7 us (8%)
  between operations  14.1 us (6%)
    all_to_all x1, blocking collectives, sum_at_owner(): lax.all_to_all(in_blocks(value, dim, length), axis, 0, 0, tiled=True)  30.4 us
    all_gather x1, blocking collectives, shards(): totals = lax.all_gather(device_total[None], 'sp', axis=0, tiled=True)  28.2 us
    all_gather x1, blocking collectives, shards(): piece = lax.all_gather(local_final[None], 'sp', axis=0, tiled=True)  25.9 us
    all_to_all x2, waiting for transfers between devices, from_everyone(): lax.all_to_all(jnp.broadcast_to(value[None], (length, *value.shape)), axi...  24.1 us
    all_to_all x2, starting transfers between devices, from_everyone(): lax.all_to_all(jnp.broadcast_to(value[None], (length, *value.shape)), axi...  24 us
    all_gather x1, waiting for transfers between devices, side_by_side(): lax.all_gather(both, axis, axis=dim, tiled=True)  12.5 us
    all_gather x1, blocking collectives, side_by_side(): lax.all_gather(both, axis, axis=dim, tiled=True)  12.3 us
    unnamed x76, local copies, waits for them, and re-layouts  12.3 us
  transfers between devices with their start and end apart: 4, of which 3 were waited for; matrix products, arithmetic and copies ran while one was open for 13% of the time, Pallas kernels for 0%

commit v1 on v0

--- a/solution.py
+++ b/solution.py
@@ -1,3 +1,4 @@
+import functools
 import jax
 import jax.numpy as jnp
 from jax import lax
@@ -6,6 +7,32 @@
 DK = 32
 DV = 64
 BLOCK = 64
+
+
+def link_cube(sheet, peer_axis):
+    inter = lax.axis_size(peer_axis)
+    placed = lax.axis_index(peer_axis)
+    by_place = []
+    arr_next, r2, after = (inter, placed, sheet.shape[0])
+    for j0 in range(arr_next):
+        by_place.append((j0, (j0 + 1) % arr_next))
+    xs_all = []
+    for j0 in range(arr_next):
+        xs_all.append((j0, (j0 - 1) % arr_next))
+    z = jnp.zeros((*sheet.shape[:0], arr_next * after, *sheet.shape[1:]), sheet.dtype)
+    z = lax.dynamic_update_slice_in_dim(z, sheet, r2 * after, axis=0)
+    state_now = arr_next // 2
+    a_now = all_values = sheet
+    for i0 in range(1, state_now + 1):
+        a_now = lax.ppermute(a_now, peer_axis, by_place)
+        z = lax.dynamic_update_slice_in_dim(z, a_now, (r2 - i0) % arr_next * after, axis=0)
+        if i0 < arr_next - state_now:
+            all_values = lax.ppermute(all_values, peer_axis, xs_all)
+            z = lax.dynamic_update_slice_in_dim(z, all_values, (r2 + i0) % arr_next * after, axis=0)
+    return z
+
+
+choose_samples_all_here = functools.partial(link_cube, peer_axis="sp")
 
 
 def side_by_side(arrays, axis, dim, along):
@@ -195,7 +222,7 @@
     before = lax.dynamic_index_in_dim(
         running_totals, sp_index, 0, False
     ) - lax.dynamic_index_in_dim(totals, sp_index, 0, False)
-    piece = lax.all_gather(local_final[None], "sp", axis=0, tiled=True)
+    piece = choose_samples_all_here(local_final[None])
     number = piece.shape[0]
     anchor = jnp.arange(number, dtype=jnp.int32)
     exponent = jnp.where(

time: 247 us -> 272 us (1.10)
  starting transfers between devices: 26.3 us -> 66.6 us
  blocking collectives: 96.8 us -> 75.9 us
    ppermute x0 -> x15, starting transfers between devices: none -> 47.7 us  [the longest x7 29.7 us: link_cube(): all_values = lax.ppermute(all_values, peer_axis, xs_all)]
    all_gather x1 -> x0, blocking collectives: 25.9 us -> none  [shards(): piece = lax.all_gather(local_final[None], 'sp', axis=0, tiled=True)]
    all_to_all x2, starting transfers between devices: 24 us -> 17.7 us  [from_everyone(): lax.all_to_all(jnp.broadcast_to(value[None], (length, *value.shape)), axi...]
    all_to_all x1, blocking collectives: 30.4 us -> 35.4 us  [sum_at_owner(): lax.all_to_all(in_blocks(value, dim, length), axis, 0, 0, tiled=True)]
    ppermute x0 -> x15, waiting for transfers between devices: none -> 3.93 us  [the longest x8 3.91 us: link_cube(): a_now = lax.ppermute(a_now, peer_axis, by_place)]
    all_to_all x2, waiting for transfers between devices: 24.1 us -> 20.7 us  [from_everyone(): lax.all_to_all(jnp.broadcast_to(value[None], (length, *value.shape)), axi...]
    unnamed x76 -> x74, local copies, waits for them, and re-layouts: 12.3 us -> 13 us
  transfers between devices with their start and end apart: 4 -> 19, of which waited for: 3 -> 3; matrix products, arithmetic and copies ran while one was open for 13% -> 19% of each run, Pallas kernels for 0% -> 0%
where the time goes in v1:
time: 272 us; the launch traced here: 270 us
  blocking collectives  75.9 us (28%)
  starting transfers between devices  66.6 us (24%)
  waiting for transfers between devices  37.2 us (14%)
  matrix products  27.7 us (10%)
  local copies, waits for them, and re-layouts  27.6 us (10%)
  other arithmetic  20.7 us (8%)
  between operations  14.3 us (5%)
    all_to_all x1, blocking collectives, sum_at_owner(): lax.all_to_all(in_blocks(value, dim, length), axis, 0, 0, tiled=True)  35.4 us
    ppermute x7, starting transfers between devices, link_cube(): all_values = lax.ppermute(all_values, peer_axis, xs_all)  29.7 us
    all_gather x1, blocking collectives, shards(): totals = lax.all_gather(device_total[None], 'sp', axis=0, tiled=True)  28.2 us
    all_to_all x2, waiting for transfers between devices, from_everyone(): lax.all_to_all(jnp.broadcast_to(value[None], (length, *value.shape)), axi...  20.7 us
    ppermute x8, starting transfers between devices, link_cube(): a_now = lax.ppermute(a_now, peer_axis, by_place)  18 us
    all_to_all x2, starting transfers between devices, from_everyone(): lax.all_to_all(jnp.broadcast_to(value[None], (length, *value.shape)), axi...  17.7 us
    unnamed x74, local copies, waits for them, and re-layouts  13 us
    all_gather x1, waiting for transfers between devices, side_by_side(): lax.all_gather(both, axis, axis=dim, tiled=True)  12.5 us
  transfers between devices with their start and end apart: 19, of which 3 were waited for; matrix products, arithmetic and copies ran while one was open for 19% of the time, Pallas kernels for 0%

profile of v1, /device:TPU:1, one launch (start us, length us, event | category | flops | bytes accessed | tf_op | source)
XLA Modules:
  0.0 270.1 jit_solution(17423819853089002096)
XLA Ops:
  7.5 12.3 %all_gather.9 = bf16[256,896]{1,0:T(8,128)(2,1)} all-gather(bf16[64,896]{1,0:T(8,128)(2,1)S(1)} %concatenate.11), channel_id=1, replica_groups=mesh['sp'=16,'fs'=4,'tp'=8] {'fs'}, dimensions={0}, use_global_device_ids=true | all-gather | bytes 573440 | tf_op jit(solution)/shard_map/all_gather | solution.py:44
  22.4 11.6 %all-to-all-start = ((bf16[8,256,512]{1,2,0:T(8,128)(2,1)}), bf16[8,256,512]{1,2,0:T(8,128)(2,1)S(1)}, u32[]{:S(2)}, u32[]{:S(2)}) async-start(bf16[8,256,512]{1,2,0:T(8,128)(2,1)} %broadcast_in_dim.47), calls=%async_computation | async-start | bytes 4194304 | tf_op jit(solution)/shard_map/all_to_all | solution.py:49
  39.6 20.7 %all-to-all-done = bf16[8,256,512]{1,2,0:T(8,128)(2,1)S(1)} async-done(((bf16[8,256,512]{1,2,0:T(8,128)(2,1)}), bf16[8,256,512]{1,2,0:T(8,128)(2,1)S(1)}, u32[]{:S(2)}, u32[]{:S(2)}) %all-to-all-start) | async-done | bytes 2097184 | tf_op jit(solution)/shard_map/all_to_all | solution.py:49
  62.6 2.2 fusion.86
  65.5 28.2 %all-gather.1 = f32[16,2,32]{2,1,0:T(2,128)S(1)} all-gather(f32[1,2,32]{2,1,0:T(2,128)S(1)} %bitcast.162), channel_id=2, replica_groups=mesh['sp'=16,'fs'=4,'tp'=8] {'sp'}, dimensions={0}, use_global_device_ids=true | all-gather | bytes 4352 | tf_op jit(solution)/shard_map/all_gather | solution.py:219
  94.0 4.5 %select_exponential_fusion = f32[4,2,64,64,32]{3,4,2,1,0:T(8,128)} fusion(f32[4,2,64,32]{2,3,1,0:T(8,128)S(1)} %copy.67, f32[4,2,64,32]{3,2,1,0:T(8,128)S(1)} %reduce_window_sum.35, pred[64,64]{1,0:T(8,128)(4,1)S(1)} %iota_compare_fusion), kind=kLoop, calls=%fused_computation.5 | loop fusion | flops 2097152 | bytes 4329472 | tf_op jit(solution)/shard_map/exp | solution.py:200
  98.5 11.0 %copy.82 = f32[4,2,64,64,32]{2,3,4,1,0:T(8,128)} copy(f32[4,2,64,64,32]{3,4,2,1,0:T(8,128)} %select_exponential_fusion) | data formatting | bytes 8388608
  109.5 12.5 %all-gather.4.cloned.1.call-done = bf16[4096,896]{1,0:T(8,128)(2,1)} async-done(((bf16[256,896]{1,0:T(8,128)(2,1)}), bf16[4096,896]{1,0:T(8,128)(2,1)}) %all-gather.4.cloned.1.call-update) | async-done | bytes 7340048 | tf_op jit(solution)/shard_map/all_gather | solution.py:44
  122.1 2.2 fusion.18
  125.3 2.0 fusion.13
  127.4 2.0 fusion.38
  129.3 5.8 %while.13 = (s32[]{:T(128)}, f32[2,32,64]{2,1,0:T(8,128)S(1)}, f32[4,2,32,64]{3,2,1,0:T(8,128)}, f32[4,2,32]{2,1,0:T(2,128)S(1)}, f32[4,2,32,64]{3,2,1,0:T(8,128)}, /*index=5*/s32[]{:T(128)}, s32[]{:T(128)}) while((s32[]{:T(128)}, f32[2,32,64]{2,1,0:T(8,128)S(1)}, f32[4,2,32,64]{3,2,1,0:T(8,128)}, f32[4,2,32]{2,1,0:T(2,128)S(1)}, ...), condition=%wide.region_9.10_spmd.clone, body=%wide.region_8.9_spmd.clone.sunk | while | flops 16387 | bytes 99680 | solution.py:215
  135.2 1.9 collective-permute-start.1
  137.1 4.6 %collective-permute-start.2 = (f32[1,2,32,64]{3,2,1,0:T(8,128)S(1)}, f32[1,2,32,64]{3,2,1,0:T(8,128)}, u32[]{:S(2)}, u32[]{:S(2)}) collective-permute-start(f32[1,2,32,64]{3,2,1,0:T(8,128)S(1)} %bitcast.153), channel_id=1, source_target_pairs={{0,480},{32,0},{64,32},{96,64},{128,96},{160,128},{192,160},{224,1... | collective-permute-start | bytes 49160 | tf_op jit(solution)/shard_map/ppermute | solution.py:30
  144.2 5.3 %fusion = f32[4,2,64,64]{2,3,1,0:T(8,128)S(1)} fusion(f32[4,2,64,64,32]{2,3,4,1,0:T(8,128)} %copy.82, f32[4,2,32,64]{3,2,1,0:T(8,128)S(1)} %copy.69, f32[4,2,32,64]{3,2,1,0:T(8,128)} %copy.68), kind=kLoop, calls=%fused_computation.4 | loop fusion | flops 3112960 | bytes 4456448 | tf_op jit(solution)/shard_map/nhid,nhjd,nhijd->nhij/dot_general | solution.py:201
  150.8 2.0 fusion.12
  152.8 2.0 fusion.6
  159.7 6.1 %all-to-all-start.1 = ((f32[8,1,512]{2,1,0:T(1,128)}), f32[8,1,512]{2,1,0:T(1,128)S(1)}, u32[]{:S(2)}, u32[]{:S(2)}) async-start(f32[8,1,512]{2,1,0:T(1,128)} %broadcast_in_dim.48), calls=%async_computation.1 | async-start | bytes 32768 | tf_op jit(solution)/shard_map/all_to_all | solution.py:49
  165.8 3.9 %collective-permute-start.3 = (f32[1,2,32,64]{3,2,1,0:T(8,128)}, f32[1,2,32,64]{3,2,1,0:T(8,128)S(1)}, u32[]{:S(2)}, u32[]{:S(2)}) collective-permute-start(f32[1,2,32,64]{3,2,1,0:T(8,128)} %collective-permute-done.1), channel_id=1, source_target_pairs={{0,32},{32,64},{64,96},{96,128},{128,160},{160,192},{192,224},{224... | collective-permute-start | bytes 49160 | tf_op jit(solution)/shard_map/ppermute | solution.py:27
  169.7 2.9 %collective-permute-start.4 = (f32[1,2,32,64]{3,2,1,0:T(8,128)}, f32[1,2,32,64]{3,2,1,0:T(8,128)S(1)}, u32[]{:S(2)}, u32[]{:S(2)}) collective-permute-start(f32[1,2,32,64]{3,2,1,0:T(8,128)} %collective-permute-done.2), channel_id=1, source_target_pairs={{0,480},{32,0},{64,32},{96,64},{128,96},{160,128},{192,160},{224,1... | collective-permute-start | bytes 49160 | tf_op jit(solution)/shard_map/ppermute | solution.py:30
  174.9 4.2 %fusion.31 = f32[4096,256]{1,0:T(8,128)} fusion(bf16[4096,896]{1,0:T(8,128)(2,1)} %all-gather.4.cloned.1.call-done, f32[256,128]{1,0:T(8,128)} %get-tuple-element.65, f32[128]{0:T(128)} %dynamic_slice.28, f32[256]{0:T(256)S(1)} %get-tuple-element.100, f32[256]{0:T(256)S(1)} %get-tuple-element.99), kind=kOutput, calls=%fused_computation.50 | convolution fusion | flops 268697600 | bytes 5376512 | tf_op jit(solution)/shard_map/dot_general | solution.py:249
  179.2 2.6 collective-permute-start.5
  181.8 3.9 %collective-permute-start.6 = (f32[1,2,32,64]{3,2,1,0:T(8,128)S(1)}, f32[1,2,32,64]{3,2,1,0:T(8,128)S(1)}, u32[]{:S(2)}, u32[]{:S(2)}) collective-permute-start(f32[1,2,32,64]{3,2,1,0:T(8,128)S(1)} %collective-permute-done.4), channel_id=1, source_target_pairs={{0,480},{32,0},{64,32},{96,64},{128,96},{160,128},{192,160},{224,1... | collective-permute-start | bytes 49160 | tf_op jit(solution)/shard_map/ppermute | solution.py:30
  185.7 1.9 collective-permute-start.7
  187.7 4.6 %collective-permute-start.8 = (f32[1,2,32,64]{3,2,1,0:T(8,128)S(1)}, f32[1,2,32,64]{3,2,1,0:T(8,128)S(1)}, u32[]{:S(2)}, u32[]{:S(2)}) collective-permute-start(f32[1,2,32,64]{3,2,1,0:T(8,128)S(1)} %collective-permute-done.6), channel_id=1, source_target_pairs={{0,480},{32,0},{64,32},{96,64},{128,96},{160,128},{192,160},{224,1... | collective-permute-start | bytes 49160 | tf_op jit(solution)/shard_map/ppermute | solution.py:30
  192.3 1.9 collective-permute-start.9
  194.2 4.6 %collective-permute-start.10 = (f32[1,2,32,64]{3,2,1,0:T(8,128)S(1)}, f32[1,2,32,64]{3,2,1,0:T(8,128)S(1)}, u32[]{:S(2)}, u32[]{:S(2)}) collective-permute-start(f32[1,2,32,64]{3,2,1,0:T(8,128)S(1)} %collective-permute-done.8), channel_id=1, source_target_pairs={{0,480},{32,0},{64,32},{96,64},{128,96},{160,128},{192,160},{224,1... | collective-permute-start | bytes 49160 | tf_op jit(solution)/shard_map/ppermute | solution.py:30
  200.8 4.6 %collective-permute-start.12 = (f32[1,2,32,64]{3,2,1,0:T(8,128)S(1)}, f32[1,2,32,64]{3,2,1,0:T(8,128)S(1)}, u32[]{:S(2)}, u32[]{:S(2)}) collective-permute-start(f32[1,2,32,64]{3,2,1,0:T(8,128)S(1)} %collective-permute-done.10), channel_id=1, source_target_pairs={{0,480},{32,0},{64,32},{96,64},{128,96},{160,128},{192,160},{224,1... | collective-permute-start | bytes 49160 | tf_op jit(solution)/shard_map/ppermute | solution.py:30
  207.4 4.6 %collective-permute-start.14 = (f32[1,2,32,64]{3,2,1,0:T(8,128)S(1)}, f32[1,2,32,64]{3,2,1,0:T(8,128)S(1)}, u32[]{:S(2)}, u32[]{:S(2)}) collective-permute-start(f32[1,2,32,64]{3,2,1,0:T(8,128)S(1)} %collective-permute-done.12), channel_id=1, source_target_pairs={{0,480},{32,0},{64,32},{96,64},{128,96},{160,128},{192,160},{224,1... | collective-permute-start | bytes 49160 | tf_op jit(solution)/shard_map/ppermute | solution.py:30
  214.0 3.9 %collective-permute-done.15 = f32[1,2,32,64]{3,2,1,0:T(8,128)S(1)} collective-permute-done((f32[1,2,32,64]{3,2,1,0:T(8,128)S(1)}, f32[1,2,32,64]{3,2,1,0:T(8,128)S(1)}, u32[]{:S(2)}, u32[]{:S(2)}) %collective-permute-start.15) | collective-permute-done | bytes 16416 | tf_op jit(solution)/shard_map/ppermute | solution.py:27
  221.0 5.7 %fusion.1 = bf16[4096,256]{1,0:T(8,128)(2,1)} fusion(f32[4096,256]{1,0:T(8,128)} %fusion.31, bf16[4096,896]{1,0:T(8,128)(2,1)} %all-gather.4.cloned.1.call-done, f32[256,128]{1,0:T(8,128)S(1)} %reshape.78, bf16[256,4096]{0,1:T(8,128)(2,1)S(1)} %copy-done.2, f32[256]{0:T(256)S(1)} %add_rsqrt_fusion.1), kind=kOutput, calls=%fused_computation.7 | convolution fusion | flops 539262976 | bytes 10617856 | tf_op jit(solution)/shard_map/dot_general | solution.py:255
  226.7 35.4 %all_to_all.16 = bf16[8,512,256]{2,1,0:T(8,128)(2,1)S(1)} all-to-all(bf16[8,512,256]{2,1,0:T(8,128)(2,1)} %bitcast.151), channel_id=1, replica_groups=mesh['sp'=16,'fs'=4,'tp'=8] {'tp'}, dimensions={0} | all-to-all | bytes 4194304 | tf_op jit(solution)/shard_map/all_to_all | solution.py:93
  (172 shorter events, 40.0 us)
Async XLA Ops:
  6.5 56.1 %copy-start = (bf16[4096,64]{0,1:T(8,128)(2,1)S(1)}, bf16[4096,64]{0,1:T(8,128)(2,1)}, u32[]{:S(2)}) copy-start(bf16[4096,64]{0,1:T(8,128)(2,1)} %param.29) | copy-start | bytes 1572868
  6.5 115.5 %all-gather.4.cloned.1.call-start = ((), (), s32[]{:S(2)}) async-start(), calls=%async_computation.3 | async-start | bytes 7798784 | tf_op jit(solution)/shard_map/all_gather | solution.py:44
  20.9 39.9 %copy-start.7 = (f32[4096]{0:T(1024)S(1)}, f32[4096]{0:T(1024)}, u32[]{:S(2)}) copy-start(f32[4096]{0:T(1024)} %param.20) | copy-start | bytes 49156
  22.4 37.8 %all-to-all-start = ((bf16[8,256,512]{1,2,0:T(8,128)(2,1)}), bf16[8,256,512]{1,2,0:T(8,128)(2,1)S(1)}, u32[]{:S(2)}, u32[]{:S(2)}) async-start(bf16[8,256,512]{1,2,0:T(8,128)(2,1)} %broadcast_in_dim.47), calls=%async_computation | async-start | bytes 4194304 | tf_op jit(solution)/shard_map/all_to_all | solution.py:49
  34.0 28.6 %copy-start.6 = (f32[1,256,64]{1,2,0:T(8,128)S(1)}, f32[1,256,64]{1,2,0:T(8,128)}, u32[]{:S(2)}) copy-start(f32[1,256,64]{1,2,0:T(8,128)} %param.32) | copy-start | bytes 196612
  98.5 23.6 %copy-start.1 = (bf16[256,4096]{0,1:T(8,128)(2,1)S(1)}, bf16[256,4096]{0,1:T(8,128)(2,1)}, u32[]{:S(2)}) copy-start(bf16[256,4096]{0,1:T(8,128)(2,1)} %fusion.2) | copy-start | bytes 6291460
  135.2 30.6 %collective-permute-start.1 = (f32[1,2,32,64]{3,2,1,0:T(8,128)S(1)}, f32[1,2,32,64]{3,2,1,0:T(8,128)}, u32[]{:S(2)}, u32[]{:S(2)}) collective-permute-start(f32[1,2,32,64]{3,2,1,0:T(8,128)S(1)} %bitcast.152), channel_id=1, source_target_pairs={{0,32},{32,64},{64,96},{96,128},{128,160},{160,192},{192,224},{224... | collective-permute-start | bytes 49160 | tf_op jit(solution)/shard_map/ppermute | solution.py:27
  137.1 32.6 %collective-permute-start.2 = (f32[1,2,32,64]{3,2,1,0:T(8,128)S(1)}, f32[1,2,32,64]{3,2,1,0:T(8,128)}, u32[]{:S(2)}, u32[]{:S(2)}) collective-permute-start(f32[1,2,32,64]{3,2,1,0:T(8,128)S(1)} %bitcast.153), channel_id=1, source_target_pairs={{0,480},{32,0},{64,32},{96,64},{128,96},{160,128},{192,160},{224,1... | collective-permute-start | bytes 49160 | tf_op jit(solution)/shard_map/ppermute | solution.py:30
  150.5 6.5 %copy-start.12 = (f32[128]{0:T(128)S(1)}, f32[128]{0:T(128)}, u32[]{:S(2)}) copy-start(f32[128]{0:T(128)} %get-tuple-element.73) | copy-start | bytes 1540
  150.6 6.5 %copy-start.13 = (f32[128]{0:T(128)S(1)}, f32[128]{0:T(128)}, u32[]{:S(2)}) copy-start(f32[128]{0:T(128)} %get-tuple-element.74) | copy-start | bytes 1540
  150.6 6.5 %copy-start.14 = (f32[128]{0:T(128)S(1)}, f32[128]{0:T(128)}, u32[]{:S(2)}) copy-start(f32[128]{0:T(128)} %get-tuple-element.75) | copy-start | bytes 1540
  150.6 6.5 %copy-start.15 = (f32[128]{0:T(128)S(1)}, f32[128]{0:T(128)}, u32[]{:S(2)}) copy-start(f32[128]{0:T(128)} %get-tuple-element.76) | copy-start | bytes 1540
  150.6 6.5 %copy-start.16 = (f32[128]{0:T(128)S(1)}, f32[128]{0:T(128)}, u32[]{:S(2)}) copy-start(f32[128]{0:T(128)} %get-tuple-element.77) | copy-start | bytes 1540
  154.8 2.2 collective-permute-start
  159.1 59.6 %copy-start.5 = (f32[4,2,64,64]{2,3,1,0:T(8,128)S(1)}, f32[4,2,64,64]{2,3,1,0:T(8,128)}, u32[]{:S(2)}) copy-start(f32[4,2,64,64]{2,3,1,0:T(8,128)} %fusion.73) | copy-start | bytes 393220
  159.1 61.4 %copy-start.35 = (f32[64]{0:T(128)S(1)}, f32[64]{0:T(128)}, u32[]{:S(2)}) copy-start(f32[64]{0:T(128)} %param.35) | copy-start | bytes 772
  159.7 14.4 %all-to-all-start.1 = ((f32[8,1,512]{2,1,0:T(1,128)}), f32[8,1,512]{2,1,0:T(1,128)S(1)}, u32[]{:S(2)}, u32[]{:S(2)}) async-start(f32[8,1,512]{2,1,0:T(1,128)} %broadcast_in_dim.48), calls=%async_computation.1 | async-start | bytes 32768 | tf_op jit(solution)/shard_map/all_to_all | solution.py:49
  165.8 13.4 %collective-permute-start.3 = (f32[1,2,32,64]{3,2,1,0:T(8,128)}, f32[1,2,32,64]{3,2,1,0:T(8,128)S(1)}, u32[]{:S(2)}, u32[]{:S(2)}) collective-permute-start(f32[1,2,32,64]{3,2,1,0:T(8,128)} %collective-permute-done.1), channel_id=1, source_target_pairs={{0,32},{32,64},{64,96},{96,128},{128,160},{160,192},{192,224},{224... | collective-permute-start | bytes 49160 | tf_op jit(solution)/shard_map/ppermute | solution.py:27
  169.7 12.0 %collective-permute-start.4 = (f32[1,2,32,64]{3,2,1,0:T(8,128)}, f32[1,2,32,64]{3,2,1,0:T(8,128)S(1)}, u32[]{:S(2)}, u32[]{:S(2)}) collective-permute-start(f32[1,2,32,64]{3,2,1,0:T(8,128)} %collective-permute-done.2), channel_id=1, source_target_pairs={{0,480},{32,0},{64,32},{96,64},{128,96},{160,128},{192,160},{224,1... | collective-permute-start | bytes 49160 | tf_op jit(solution)/shard_map/ppermute | solution.py:30
  174.9 10.7 %copy-start.4 = (f32[16,2,32,64]{3,2,1,0:T(8,128)S(1)}, f32[16,2,32,64]{3,2,1,0:T(8,128)}, u32[]{:S(2)}) copy-start(f32[16,2,32,64]{3,2,1,0:T(8,128)} %copy-done.3) | copy-start | bytes 786436
  174.9 46.0 %copy-start.2 = (bf16[256,4096]{0,1:T(8,128)(2,1)S(1)}, bf16[256,4096]{0,1:T(8,128)(2,1)}, u32[]{:S(2)}) copy-start(bf16[256,4096]{0,1:T(8,128)(2,1)} %fusion.2) | copy-start | bytes 6291460
  179.2 6.6 %collective-permute-start.5 = (f32[1,2,32,64]{3,2,1,0:T(8,128)S(1)}, f32[1,2,32,64]{3,2,1,0:T(8,128)S(1)}, u32[]{:S(2)}, u32[]{:S(2)}) collective-permute-start(f32[1,2,32,64]{3,2,1,0:T(8,128)S(1)} %collective-permute-done.3), channel_id=1, source_target_pairs={{0,32},{32,64},{64,96},{96,128},{128,160},{160,192},{192,224},{224... | collective-permute-start | bytes 49160 | tf_op jit(solution)/shard_map/ppermute | solution.py:27
  181.8 5.9 %collective-permute-start.6 = (f32[1,2,32,64]{3,2,1,0:T(8,128)S(1)}, f32[1,2,32,64]{3,2,1,0:T(8,128)S(1)}, u32[]{:S(2)}, u32[]{:S(2)}) collective-permute-start(f32[1,2,32,64]{3,2,1,0:T(8,128)S(1)} %collective-permute-done.4), channel_id=1, source_target_pairs={{0,480},{32,0},{64,32},{96,64},{128,96},{160,128},{192,160},{224,1... | collective-permute-start | bytes 49160 | tf_op jit(solution)/shard_map/ppermute | solution.py:30
  185.7 6.6 %collective-permute-start.7 = (f32[1,2,32,64]{3,2,1,0:T(8,128)S(1)}, f32[1,2,32,64]{3,2,1,0:T(8,128)S(1)}, u32[]{:S(2)}, u32[]{:S(2)}) collective-permute-start(f32[1,2,32,64]{3,2,1,0:T(8,128)S(1)} %collective-permute-done.5), channel_id=1, source_target_pairs={{0,32},{32,64},{64,96},{96,128},{128,160},{160,192},{192,224},{224... | collective-permute-start | bytes 49160 | tf_op jit(solution)/shard_map/ppermute | solution.py:27
  187.7 6.6 %collective-permute-start.8 = (f32[1,2,32,64]{3,2,1,0:T(8,128)S(1)}, f32[1,2,32,64]{3,2,1,0:T(8,128)S(1)}, u32[]{:S(2)}, u32[]{:S(2)}) collective-permute-start(f32[1,2,32,64]{3,2,1,0:T(8,128)S(1)} %collective-permute-done.6), channel_id=1, source_target_pairs={{0,480},{32,0},{64,32},{96,64},{128,96},{160,128},{192,160},{224,1... | collective-permute-start | bytes 49160 | tf_op jit(solution)/shard_map/ppermute | solution.py:30
  192.3 6.6 %collective-permute-start.9 = (f32[1,2,32,64]{3,2,1,0:T(8,128)S(1)}, f32[1,2,32,64]{3,2,1,0:T(8,128)S(1)}, u32[]{:S(2)}, u32[]{:S(2)}) collective-permute-start(f32[1,2,32,64]{3,2,1,0:T(8,128)S(1)} %collective-permute-done.7), channel_id=1, source_target_pairs={{0,32},{32,64},{64,96},{96,128},{128,160},{160,192},{192,224},{224... | collective-permute-start | bytes 49160 | tf_op jit(solution)/shard_map/ppermute | solution.py:27
  194.2 6.6 %collective-permute-start.10 = (f32[1,2,32,64]{3,2,1,0:T(8,128)S(1)}, f32[1,2,32,64]{3,2,1,0:T(8,128)S(1)}, u32[]{:S(2)}, u32[]{:S(2)}) collective-permute-start(f32[1,2,32,64]{3,2,1,0:T(8,128)S(1)} %collective-permute-done.8), channel_id=1, source_target_pairs={{0,480},{32,0},{64,32},{96,64},{128,96},{160,128},{192,160},{224,1... | collective-permute-start | bytes 49160 | tf_op jit(solution)/shard_map/ppermute | solution.py:30
  198.9 6.6 %collective-permute-start.11 = (f32[1,2,32,64]{3,2,1,0:T(8,128)S(1)}, f32[1,2,32,64]{3,2,1,0:T(8,128)S(1)}, u32[]{:S(2)}, u32[]{:S(2)}) collective-permute-start(f32[1,2,32,64]{3,2,1,0:T(8,128)S(1)} %collective-permute-done.9), channel_id=1, source_target_pairs={{0,32},{32,64},{64,96},{96,128},{128,160},{160,192},{192,224},{224... | collective-permute-start | bytes 49160 | tf_op jit(solution)/shard_map/ppermute | solution.py:27
  200.8 6.6 %collective-permute-start.12 = (f32[1,2,32,64]{3,2,1,0:T(8,128)S(1)}, f32[1,2,32,64]{3,2,1,0:T(8,128)S(1)}, u32[]{:S(2)}, u32[]{:S(2)}) collective-permute-start(f32[1,2,32,64]{3,2,1,0:T(8,128)S(1)} %collective-permute-done.10), channel_id=1, source_target_pairs={{0,480},{32,0},{64,32},{96,64},{128,96},{160,128},{192,160},{224,1... | collective-permute-start | bytes 49160 | tf_op jit(solution)/shard_map/ppermute | solution.py:30
  205.4 6.6 %collective-permute-start.13 = (f32[1,2,32,64]{3,2,1,0:T(8,128)S(1)}, f32[1,2,32,64]{3,2,1,0:T(8,128)S(1)}, u32[]{:S(2)}, u32[]{:S(2)}) collective-permute-start(f32[1,2,32,64]{3,2,1,0:T(8,128)S(1)} %collective-permute-done.11), channel_id=1, source_target_pairs={{0,32},{32,64},{64,96},{96,128},{128,160},{160,192},{192,224},{224... | collective-permute-start | bytes 49160 | tf_op jit(solution)/shard_map/ppermute | solution.py:27
  207.4 6.6 %collective-permute-start.14 = (f32[1,2,32,64]{3,2,1,0:T(8,128)S(1)}, f32[1,2,32,64]{3,2,1,0:T(8,128)S(1)}, u32[]{:S(2)}, u32[]{:S(2)}) collective-permute-start(f32[1,2,32,64]{3,2,1,0:T(8,128)S(1)} %collective-permute-done.12), channel_id=1, source_target_pairs={{0,480},{32,0},{64,32},{96,64},{128,96},{160,128},{192,160},{224,1... | collective-permute-start | bytes 49160 | tf_op jit(solution)/shard_map/ppermute | solution.py:30
  212.0 5.9 %collective-permute-start.15 = (f32[1,2,32,64]{3,2,1,0:T(8,128)S(1)}, f32[1,2,32,64]{3,2,1,0:T(8,128)S(1)}, u32[]{:S(2)}, u32[]{:S(2)}) collective-permute-start(f32[1,2,32,64]{3,2,1,0:T(8,128)S(1)} %collective-permute-done.13), channel_id=1, source_target_pairs={{0,32},{32,64},{64,96},{96,128},{128,160},{160,192},{192,224},{224... | collective-permute-start | bytes 49160 | tf_op jit(solution)/shard_map/ppermute | solution.py:27
  (23 other events, 144.0 us)
Sparse Core Ops, SparseCore 0:
  20.0 102.0 all-gather.3
